TPU v7x, 512 devices: a 4x2x32 block of a 4x8x32 slice. The times are simulated.
512 devices in a mesh: grp: 2 (over y), kv: 32 (over z), tp: 8 (over x, core).
Axes of the slice: x: 4, y: 2, z: 32, core: 2. Of those that a mesh axis runs over, the one named last changes fastest.
The devices are a block of a 4x8x32 slice.
Arguments:
- tokens: bfloat16 [256, 4096], P('grp', 'kv'), parts along dimension 0, may hold values from -100 to 100
- norm_gain: bfloat16 [4096], P('kv'), may hold values from 0.099609375 to 1.8984375
- w_query1: bfloat16 [4096, 1024], P('kv', 'tp'), may hold values from -0.15625 to 0.15625
- w_query2: bfloat16 [4096, 1024], P('kv', 'tp'), may hold values from -0.15625 to 0.15625
- w_key1: bfloat16 [4096, 1024], P('kv', 'tp'), may hold values from -0.09375 to 0.09375
- w_key2: bfloat16 [4096, 1024], P('kv', 'tp'), may hold values from -0.09375 to 0.09375
- w_value: bfloat16 [4096, 2048], P('kv', 'tp'), may hold values from -0.09375 to 0.09375
- head_gain: bfloat16 [128], replicated, may hold values from 0.099609375 to 1.8984375
- lambdas: float32 [16], P('tp'), may hold values from 0.3 to 0.8
- w_out: bfloat16 [2048, 4096], P('tp', 'kv'), may hold values from -0.125 to 0.125
- cache_keys: bfloat16 [16, 8192, 16, 128], P('grp', 'kv', 'tp'), parts along dimension 0, may hold values from -330 to 330
- cache_values: bfloat16 [16, 8192, 16, 128], P('grp', 'kv', 'tp'), parts along dimension 0, may hold values from -6 to 6
- lengths: int32 [16], P('grp'), parts along dimension 0, may hold values from 4096 to 8160
- accepted: int32 [16], P('grp'), parts along dimension 0, may hold values from 0 to 16
- parents: int32 [16, 16], P('grp'), parts along dimension 0, may hold values from -1 to 14, as said below
Outputs:
- mixed: bfloat16 [256, 4096], P(('grp', 'tp'), 'kv'), parts along dimension 0
- new_keys: bfloat16 [16, 8192, 16, 128], P('grp', 'kv', 'tp'), parts along dimension 0
- new_values: bfloat16 [16, 8192, 16, 128], P('grp', 'kv', 'tp'), parts along dimension 0
There are 2 independent parts, one for each index of `grp`. A program takes and returns all parts, laid end to end along the dimension named above; an argument that names none is the same for every part. Nothing has to cross between parts.
Inputs may be any that keep to these rules, and one draw needn't show every extreme that they name: parents[s, 0] = -1; for j of 1 onward parents[s, j] lies between 0 and j - 1.
All inputs are finite; a program needn't handle non-finite values.
Results may differ from a plain program's by a relative error of at most 0.01225.
The roundings to bfloat16 on the way count: a program that leaves them out, or rounds other values in their place, can miss the bound.
Values may be sent and summed in bfloat16 or wider, within the bound.
No kernel may reach another device: no remote copies, remote signals or barrier semaphores. Data moves between devices by JAX's collectives and lax.ppermute only.
A program may use at most 64 MiB of HBM per device.

v0:
```python
import math

import jax
import jax.numpy as jnp
from jax import lax
from jax.sharding import PartitionSpec as P

D = 4096


epsilon = 1e-06
masked_fill = -1e30
head_factor = 0.8


def split_up(shard, dim, devices):
    dims = shard.shape
    pieces = shard.reshape(*dims[:dim], devices, dims[dim] // devices, *dims[dim + 1 :])
    return jnp.moveaxis(pieces, dim, 0)


def sum_at_owner(shard, axis, dim):
    devices = lax.axis_size(axis)
    pieces = lax.all_to_all(split_up(shard, dim, devices), axis, 0, 0, tiled=True)
    return jnp.sum(pieces, axis=0)


def side_by_side(arrays, axis, dim, along):
    widths = [math.prod(a.shape[along:]) for a in arrays]
    both = jnp.concatenate(
        [a.reshape(*a.shape[:along], w) for a, w in zip(arrays, widths)], axis=along
    )
    whole = sum_at_owner(both, axis, dim)
    pieces = jnp.split(whole, [sum(widths[:k]) for k in range(1, len(widths))], axis=along)
    return tuple(
        (b.reshape(*whole.shape[:along], *a.shape[along:]) for a, b in zip(arrays, pieces))
    )


def from_everyone(shard, axis):
    copies = jnp.broadcast_to(shard, (lax.axis_size(axis), *shard.shape))
    return lax.all_to_all(copies, axis, split_axis=0, concat_axis=0, tiled=True)


def in_order(pieces, dim):
    dims = list(pieces.shape[1:])
    dims[dim] *= pieces.shape[0]
    return jnp.moveaxis(pieces, 0, dim).reshape(dims)


def collect(shard, axis, dim):
    pieces = from_everyone(shard, axis)
    return in_order(pieces, dim)


def side_by_side_2(arrays, axis, split_dim, concat_dim, along):
    widths = [math.prod(a.shape[along:]) for a in arrays]
    both = jnp.concatenate(
        [a.reshape(*a.shape[:along], w) for a, w in zip(arrays, widths)], axis=along
    )
    whole = lax.all_to_all(both, axis, split_axis=split_dim, concat_axis=concat_dim, tiled=True)
    pieces = jnp.split(whole, [sum(widths[:k]) for k in range(1, len(widths))], axis=along)
    return tuple(
        (b.reshape(*whole.shape[:along], *a.shape[along:]) for a, b in zip(arrays, pieces))
    )


def summed_on_arrival(shard, axis, dim):
    pieces = split_up(shard, dim, lax.axis_size(axis))
    arrived = lax.all_to_all(pieces, axis, split_axis=0, concat_axis=0, tiled=True)
    return arrived.astype(jnp.float32).sum(axis=0)


def ancestor_mask(parents, width):
    nodes = jnp.arange(width, dtype=jnp.int32)
    closure = (parents[:, :, None] == nodes[None, None, :]).astype(jnp.float32)
    closure = closure + jnp.eye(width, dtype=jnp.float32)[None]
    for repeat in range(width.bit_length()):
        closure = jnp.minimum(jnp.einsum("sji,sik->sjk", closure, closure), 1.0)
    return closure > 0.5


def softmax_terms(scores, visible, values):
    scores = jnp.where(visible, scores, masked_fill)
    maxima = jnp.max(scores, axis=-1)
    weights = jnp.where(visible, jnp.exp(scores - maxima[..., None]), 0.0)
    totals = jnp.sum(weights, axis=-1)
    weighted = jnp.einsum(
        "sjhp,sphe->sjhe", weights.astype(jnp.bfloat16), values, preferred_element_type=jnp.float32
    )
    return (maxima, totals, weighted)


def join_pair(first, second):
    highest = jnp.maximum(first[0], second[0])
    scale_first = jnp.exp(first[0] - highest)
    scale_second = jnp.exp(second[0] - highest)
    totals = first[1] * scale_first + second[1] * scale_second
    weighted = first[2] * scale_first[..., None] + second[2] * scale_second[..., None]
    return (highest, totals, weighted)


def join_parts(first, second):
    return join_pair(first[0:3], second[0:3]) + join_pair(first[3:6], second[3:6])


def fold_shards(parts):
    folded = ()
    for start_at in (0, 3):
        maxima = parts[start_at]
        highest = jnp.max(maxima, axis=0)
        factor = jnp.exp(maxima - highest[None])
        totals = jnp.sum(factor * parts[start_at + 1], axis=0)
        weighted = jnp.sum(factor[..., None] * parts[start_at + 2], axis=0)
        folded = folded + (highest, totals, weighted)
    return folded


def finish_heads(parts, lambdas, head_gain):
    attention_one = parts[2] / parts[1][..., None]
    attention_two = parts[5] / parts[4][..., None]
    differ = attention_one - lambdas[None, :, None] * attention_two
    normed = differ * lax.rsqrt(jnp.mean(differ * differ, axis=-1, keepdims=True) + epsilon)
    normed = normed * head_gain.astype(jnp.float32) * head_factor
    return normed.astype(jnp.bfloat16).reshape(differ.shape[0], differ.shape[1] * differ.shape[2])


def per_device(
    tokens,
    norm_gain,
    w_query1,
    w_query2,
    w_key1,
    w_key2,
    w_value,
    head_gain,
    lambdas,
    w_out,
    cache_keys,
    cache_values,
    lengths,
    accepted,
    parents,
):
    seq_count = cache_keys.shape[0]
    ctx_local = cache_keys.shape[1]
    head_local = cache_keys.shape[2]
    prop_count = parents.shape[1]
    token_count = tokens.shape[0]
    qk_size = w_query1.shape[1] // head_local
    value_size = cache_values.shape[3]
    query_cols = head_local * qk_size
    wide_tokens = tokens.astype(jnp.float32)
    scaled = (wide_tokens * norm_gain.astype(jnp.float32)[None, :]).astype(jnp.bfloat16)
    squares = jnp.sum(wide_tokens * wide_tokens, axis=1)
    partial_value = jnp.concatenate(
        [
            jnp.dot(scaled, weight, preferred_element_type=jnp.float32)
            for weight in (w_query1, w_query2, w_key1, w_key2, w_value)
        ],
        axis=1,
    )
    factors = jnp.concatenate(
        [
            jnp.full((2 * query_cols,), qk_size ** (-0.5), jnp.float32),
            jnp.ones((partial_value.shape[1] - 2 * query_cols,), jnp.float32),
        ]
    )
    sums, square_sums = side_by_side((partial_value, squares), "kv", 0, 1)
    inverse_rms = lax.rsqrt(square_sums / D + epsilon)
    projected = collect(
        (sums * inverse_rms[:, None] * factors[None, :]).astype(jnp.bfloat16), "kv", 0
    )
    layout = (seq_count, prop_count, head_local, qk_size)
    query_one = projected[:, 0:query_cols].reshape(layout)
    query_two = projected[:, query_cols : 2 * query_cols].reshape(layout)
    key_one = projected[:, 2 * query_cols : 3 * query_cols].reshape(layout)
    key_two = projected[:, 3 * query_cols : 4 * query_cols].reshape(layout)
    fresh_values = projected[:, 4 * query_cols :].reshape(
        seq_count, prop_count, head_local, value_size
    )
    fresh_keys = jnp.concatenate([key_one, key_two], axis=-1)
    valid_len = lengths + accepted
    positions = lax.axis_index("kv") * ctx_local + jnp.arange(ctx_local, dtype=jnp.int32)
    cache_visible = (positions[None, :] < valid_len[:, None])[:, None, None, :]
    tree_visible = ancestor_mask(parents, prop_count)[:, :, None, :]

    def both_maps(key_first, key_second, visible, values):
        results = ()
        for queries, key_part in ((query_one, key_first), (query_two, key_second)):
            scores = jnp.einsum(
                "sjhd,sphd->sjhp", queries, key_part, preferred_element_type=jnp.float32
            )
            results = results + softmax_terms(scores, visible, values)
        return tuple((member.reshape((token_count,) + member.shape[2:]) for member in results))

    cache_parts = both_maps(
        cache_keys[..., :qk_size], cache_keys[..., qk_size:], cache_visible, cache_values
    )
    tree_parts = both_maps(key_one, key_two, tree_visible, fresh_values)
    received = side_by_side_2(
        (
            cache_parts[0][None],
            cache_parts[1][None],
            cache_parts[2][None],
            cache_parts[3][None],
            cache_parts[4][None],
            cache_parts[5][None],
        ),
        "kv",
        1,
        0,
        3,
    )
    row_count = token_count // lax.axis_size("kv")
    row_start = lax.axis_index("kv") * row_count
    own_tree = tuple(
        (lax.dynamic_slice_in_dim(member, row_start, row_count, 0) for member in tree_parts)
    )
    own_rows = finish_heads(join_parts(fold_shards(received), own_tree), lambdas, head_gain)
    head_out = collect(own_rows, "kv", 0)
    mixed = summed_on_arrival(
        jnp.dot(head_out, w_out, preferred_element_type=jnp.float32).astype(jnp.bfloat16), "tp", 0
    ).astype(jnp.bfloat16)
    offsets = positions[None, :] - valid_len[:, None]
    proposal_ids = jnp.arange(prop_count, dtype=jnp.int32)
    picker = (offsets[:, :, None] == proposal_ids[None, None, :]).astype(jnp.bfloat16)
    landed = ((offsets >= 0) & (offsets < prop_count))[:, :, None, None]
    placed_keys = jnp.einsum(
        "scp,sphd->schd", picker, fresh_keys, preferred_element_type=jnp.float32
    ).astype(jnp.bfloat16)
    placed_values = jnp.einsum(
        "scp,sphd->schd", picker, fresh_values, preferred_element_type=jnp.float32
    ).astype(jnp.bfloat16)
    new_keys = jnp.where(landed, placed_keys, cache_keys)
    new_values = jnp.where(landed, placed_values, cache_values)
    return (mixed, new_keys, new_values)


def solution(mesh):
    return jax.shard_map(
        per_device,
        mesh=mesh,
        in_specs=(
            P("grp", "kv"),
            P("kv"),
            P("kv", "tp"),
            P("kv", "tp"),
            P("kv", "tp"),
            P("kv", "tp"),
            P("kv", "tp"),
            P(),
            P("tp"),
            P("tp", "kv"),
            P("grp", "kv", "tp", None),
            P("grp", "kv", "tp", None),
            P("grp"),
            P("grp"),
            P("grp", None),
        ),
        out_specs=(P(("grp", "tp"), "kv"), P("grp", "kv", "tp", None), P("grp", "kv", "tp", None)),
        check_vma=False,
    )
```

profile of v0, /device:TPU:33, one launch (start us, length us, event | category | flops | bytes accessed | tf_op | source)
XLA Modules:
  0.0 260.8 jit_solution(16693142222383568251)
XLA Ops:
  0.6 0.7 convert_element_type.53
  1.3 0.9 fusion.33
  2.2 0.9 fusion.68
  3.1 0.9 fusion.66
  4.0 0.9 fusion.64
  5.0 0.9 fusion.62
  5.9 0.9 fusion.60
  6.8 0.2 concatenate.31
  7.3 104.2 %all_to_all.32 = f32[32,4,769]{2,1,0:T(4,128)S(1)} all-to-all(f32[32,4,769]{2,1,0:T(4,128)S(1)} %constant_dynamic-update-slice_fusion), channel_id=1, replica_groups=mesh['grp'=2,'kv'=32,'tp'=8] {'kv'}, dimensions={0} | all-to-all | bytes 787456 | tf_op jit(solution)/shard_map/all_to_all | solution.py:24
  111.8 0.7 broadcast_in_dim.103
  112.5 5.4 %all-to-all-start.1 = ((bf16[32,4,768]{2,1,0:T(4,128)(2,1)}), bf16[32,4,768]{2,1,0:T(4,128)(2,1)}, u32[]{:S(2)}, u32[]{:S(2)}) async-start(bf16[32,4,768]{2,1,0:T(4,128)(2,1)} %broadcast_in_dim.103), calls=%async_computation.1 | async-start | bytes 393216 | tf_op jit(solution)/shard_map/all_to_all | solution.py:42
  118.1 1.9 fusion.101
  120.0 30.7 %all-to-all-done.1 = bf16[32,4,768]{2,1,0:T(4,128)(2,1)} async-done(((bf16[32,4,768]{2,1,0:T(4,128)(2,1)}), bf16[32,4,768]{2,1,0:T(4,128)(2,1)}, u32[]{:S(2)}, u32[]{:S(2)}) %all-to-all-start.1) | async-done | bytes 196640 | tf_op jit(solution)/shard_map/all_to_all | solution.py:42
  150.7 1.0 reshape.191
  151.7 0.6 fusion.103
  152.4 0.8 reshape.193
  153.3 0.5 fusion.106
  153.7 0.5 fusion.107
  154.2 0.3 copy-done.7
  154.5 0.3 convolution_bitcast_fusion.4
  154.8 0.3 fusion.14
  155.1 0.3 convolution_bitcast_fusion.5
  155.9 0.3 concatenate.29
  156.2 1.1 copy.348
  157.3 6.0 %all-to-all-start.2 = ((f32[1,128,2,260]{3,2,0,1:T(2,128)}), f32[1,128,2,260]{3,2,0,1:T(2,128)S(1)}, u32[]{:S(2)}, u32[]{:S(2)}) async-start(f32[1,128,2,260]{3,2,0,1:T(2,128)} %copy.348), calls=%async_computation.2 | async-start | bytes 786432 | tf_op jit(solution)/shard_map/all_to_all | solution.py:61
  163.4 0.2 convolution_minimum_fusion.4
  163.6 0.3 convolution_minimum_fusion.2
  163.9 0.3 fusion.6
  164.4 0.2 fusion.104
  164.7 0.2 convolution_bitcast_fusion.2
  165.1 0.2 fusion.105
  165.4 0.2 convolution_bitcast_fusion
  166.0 45.4 %all-to-all-done.2 = f32[1,128,2,260]{3,2,0,1:T(2,128)S(1)} async-done(((f32[1,128,2,260]{3,2,0,1:T(2,128)}), f32[1,128,2,260]{3,2,0,1:T(2,128)S(1)}, u32[]{:S(2)}, u32[]{:S(2)}) %all-to-all-start.2) | async-done | bytes 266272 | tf_op jit(solution)/shard_map/all_to_all | solution.py:61
  211.4 0.6 fusion.102
  213.0 0.2 fusion.78
  213.3 0.2 fusion.76
  213.6 0.6 fusion.18
  214.3 0.2 multiply_reduce_fusion
  214.6 0.7 broadcast_in_dim.110
  215.2 7.6 %all-to-all-start.3 = ((bf16[32,4,256]{2,1,0:T(4,128)(2,1)}), bf16[32,4,256]{2,1,0:T(4,128)(2,1)S(1)}, u32[]{:S(2)}, u32[]{:S(2)}) async-start(bf16[32,4,256]{2,1,0:T(4,128)(2,1)} %broadcast_in_dim.110), calls=%async_computation.3 | async-start | bytes 131072 | tf_op jit(solution)/shard_map/all_to_all | solution.py:42
  223.0 1.9 fusion.1
  224.9 20.7 %all-to-all-done.3 = bf16[32,4,256]{2,1,0:T(4,128)(2,1)S(1)} async-done(((bf16[32,4,256]{2,1,0:T(4,128)(2,1)}), bf16[32,4,256]{2,1,0:T(4,128)(2,1)S(1)}, u32[]{:S(2)}, u32[]{:S(2)}) %all-to-all-start.3) | async-done | bytes 65568 | tf_op jit(solution)/shard_map/all_to_all | solution.py:42
  245.6 0.8 convolution_convert_fusion.2
  246.3 8.8 %all-to-all-start.4 = ((bf16[8,16,128]{2,1,0:T(8,128)(2,1)}), bf16[8,16,128]{2,1,0:T(8,128)(2,1)S(1)}, u32[]{:S(2)}, u32[]{:S(2)}) async-start(bf16[8,16,128]{2,1,0:T(8,128)(2,1)} %bitcast.27), calls=%async_computation.4 | async-start | bytes 65536 | tf_op jit(solution)/shard_map/all_to_all | solution.py:70
  255.1 0.9 fusion
  256.1 2.0 copy.387
  258.1 2.0 copy.388
  260.2 0.6 reduce_sum.122
  (83 shorter events, 3.6 us)
Async XLA Ops:
  0.6 5.2 %copy-start = (bf16[128,256]{1,0:T(8,128)(2,1)S(1)}, bf16[128,256]{1,0:T(8,128)(2,1)}, u32[]{:S(2)}) copy-start(bf16[128,256]{1,0:T(8,128)(2,1)} %param.21) | copy-start | bytes 196612
  7.1 104.6 %copy-start.5 = (f32[768]{0:T(1024)S(1)}, f32[768]{0:T(1024)}, u32[]{:S(2)}) copy-start(f32[768]{0:T(1024)} %constant.11.clone.1) | copy-start | bytes 9220
  7.2 110.7 %copy-start.9 = (s32[8]{0:T(128)S(1)}, s32[8]{0:T(128)}, u32[]{:S(2)}) copy-start(s32[8]{0:T(128)} %param.27) | copy-start | bytes 100
  7.2 110.7 %copy-start.10 = (s32[8]{0:T(128)S(1)}, s32[8]{0:T(128)}, u32[]{:S(2)}) copy-start(s32[8]{0:T(128)} %param.28) | copy-start | bytes 100
  7.3 110.8 %copy-start.1 = (bf16[8,256,2,128]{3,2,1,0:T(2,128)(2,1)S(1)}, bf16[8,256,2,128]{3,2,1,0:T(2,128)(2,1)}, u32[]{:S(2)}) copy-start(bf16[8,256,2,128]{3,2,1,0:T(2,128)(2,1)} %param.25) | copy-start | bytes 3145732
  112.5 38.2 %all-to-all-start.1 = ((bf16[32,4,768]{2,1,0:T(4,128)(2,1)}), bf16[32,4,768]{2,1,0:T(4,128)(2,1)}, u32[]{:S(2)}, u32[]{:S(2)}) async-start(bf16[32,4,768]{2,1,0:T(4,128)(2,1)} %broadcast_in_dim.103), calls=%async_computation.1 | async-start | bytes 393216 | tf_op jit(solution)/shard_map/all_to_all | solution.py:42
  153.3 1.2 copy-start.7
  156.2 7.2 %copy-start.8 = (s32[8,16]{1,0:T(8,128)S(1)}, s32[8,16]{1,0:T(8,128)}, u32[]{:S(2)}) copy-start(s32[8,16]{1,0:T(8,128)} %param.29) | copy-start | bytes 1540
  156.2 8.1 %copy-start.11 = (bf16[128]{0:T(256)(128)(2,1)S(1)}, bf16[128]{0:T(256)(128)(2,1)}, u32[]{:S(2)}) copy-start(bf16[128]{0:T(256)(128)(2,1)} %param.22) | copy-start | bytes 772
  156.2 8.1 %copy-start.3 = (bf16[128,128]{1,0:T(8,128)(2,1)S(1)}, bf16[128,128]{1,0:T(8,128)(2,1)}, u32[]{:S(2)}) copy-start(bf16[128,128]{1,0:T(8,128)(2,1)} %get-tuple-element.52) | copy-start | bytes 98308
  157.3 54.1 %all-to-all-start.2 = ((f32[1,128,2,260]{3,2,0,1:T(2,128)}), f32[1,128,2,260]{3,2,0,1:T(2,128)S(1)}, u32[]{:S(2)}, u32[]{:S(2)}) async-start(f32[1,128,2,260]{3,2,0,1:T(2,128)} %copy.348), calls=%async_computation.2 | async-start | bytes 786432 | tf_op jit(solution)/shard_map/all_to_all | solution.py:61
  163.3 1.7 copy-start.2
  211.4 2.9 %copy-start.6 = (f32[2]{0:T(128)S(1)}, f32[2]{0:T(128)}, u32[]{:S(2)}) copy-start(f32[2]{0:T(128)} %param.23) | copy-start | bytes 28
  215.2 30.3 %all-to-all-start.3 = ((bf16[32,4,256]{2,1,0:T(4,128)(2,1)}), bf16[32,4,256]{2,1,0:T(4,128)(2,1)S(1)}, u32[]{:S(2)}, u32[]{:S(2)}) async-start(bf16[32,4,256]{2,1,0:T(4,128)(2,1)} %broadcast_in_dim.110), calls=%async_computation.3 | async-start | bytes 131072 | tf_op jit(solution)/shard_map/all_to_all | solution.py:42
  222.9 22.6 %copy-start.4 = (bf16[256,128]{1,0:T(8,128)(2,1)S(1)}, bf16[256,128]{1,0:T(8,128)(2,1)}, u32[]{:S(2)}) copy-start(bf16[256,128]{1,0:T(8,128)(2,1)} %param.24) | copy-start | bytes 196612
  246.3 13.8 %all-to-all-start.4 = ((bf16[8,16,128]{2,1,0:T(8,128)(2,1)}), bf16[8,16,128]{2,1,0:T(8,128)(2,1)S(1)}, u32[]{:S(2)}, u32[]{:S(2)}) async-start(bf16[8,16,128]{2,1,0:T(8,128)(2,1)} %bitcast.27), calls=%async_computation.4 | async-start | bytes 65536 | tf_op jit(solution)/shard_map/all_to_all | solution.py:70
where the time goes:
time: 262 us; the launch traced here: 261 us
  blocking collectives  104 us (40%)
  waiting for transfers between devices  96.8 us (37%)
  starting transfers between devices  27.8 us (11%)
  local copies, waits for them, and re-layouts  14.5 us (6%)
  matrix products  11.2 us (4%)
  other arithmetic  4.97 us (2%)
    all_to_all x1, blocking collectives, sum_at_owner(): lax.all_to_all(split_up(shard, dim, devices), axis, 0, 0, tiled=True)  104 us
    all_to_all x2, waiting for transfers between devices, from_everyone(): return lax.all_to_all(copies, axis, split_axis=0, concat_axis=0, tiled=True)  51.4 us
    all_to_all x1, waiting for transfers between devices, side_by_side_2(): lax.all_to_all(both, axis, split_axis=split_dim, concat_axis=concat_dim,...  45.4 us
    all_to_all x2, starting transfers between devices, from_everyone(): return lax.all_to_all(copies, axis, split_axis=0, concat_axis=0, tiled=True)  13 us
    all_to_all x1, starting transfers between devices, summed_on_arrival(): lax.all_to_all(pieces, axis, split_axis=0, concat_axis=0, tiled=True)  8.81 us
    all_to_all x1, starting transfers between devices, side_by_side_2(): lax.all_to_all(both, axis, split_axis=split_dim, concat_axis=concat_dim,...  6.04 us
  transfers between devices with their start and end apart: 4, of which 3 were waited for; matrix products, arithmetic and copies ran while one was open for 4% of the time, Pallas kernels for 0%

commit v1 on v0

v1 whole, which is shorter than its diff:
```python
import functools

import jax
import jax.numpy as jnp
from jax import lax
from jax.experimental import pallas as pl
from jax.experimental.pallas import tpu as pltpu
from jax.sharding import PartitionSpec as P

epsilon = 1e-06
masked_fill = -1e30
head_factor = 0.8
LANES = 128
ROWS = 8

f32 = jnp.float32
bf16 = jnp.bfloat16
VMEM = pl.BlockSpec(memory_space=pltpu.VMEM)
SMEM = pl.BlockSpec(memory_space=pltpu.SMEM)


def call(body, out_shape, in_specs, name, flops, out_specs=VMEM, scratch=()):
    return pl.pallas_call(
        body,
        out_shape=out_shape,
        in_specs=in_specs,
        out_specs=out_specs,
        scratch_shapes=scratch,
        cost_estimate=pl.CostEstimate(flops=flops, bytes_accessed=1 << 16, transcendentals=0),
        name=name,
    )


def shape(dims, dtype):
    return jax.ShapeDtypeStruct(dims, dtype)


def lane_iota(dims):
    return lax.broadcasted_iota(jnp.int32, dims, len(dims) - 1)


def row_iota(dims):
    return lax.broadcasted_iota(jnp.int32, dims, len(dims) - 2)


def scale_tokens(tokens_ref, gain_ref):
    wide = tokens_ref[...].astype(f32)
    return wide, (wide * gain_ref[...].astype(f32)).astype(bf16)


def by_head(first, second, head):
    half = LANES // 2
    left = first[:, head * half : (head + 1) * half]
    right = second[:, head * half : (head + 1) * half]
    return jnp.concatenate([left, right], axis=1)


def query_parts(heads, tokens_ref, gain_ref, w1_ref, w2_ref, out_ref):
    wide, scaled = scale_tokens(tokens_ref, gain_ref)
    first = jnp.dot(scaled, w1_ref[...], preferred_element_type=f32)
    second = jnp.dot(scaled, w2_ref[...], preferred_element_type=f32)
    squares = jnp.sum(jnp.transpose(wide * wide), axis=0, keepdims=True)
    for head in range(heads):
        columns = by_head(first, second, head)
        for group in range(wide.shape[0] // ROWS):
            owner = group * heads + head
            for row in range(ROWS):
                at = group * ROWS + row
                out_ref[owner, :, row * LANES : (row + 1) * LANES] = columns[at : at + 1, :]
            out_ref[owner, :, ROWS * LANES :] = squares


def value_parts(heads, tokens_ref, gain_ref, w1_ref, w2_ref, wv_ref, out_ref):
    _, scaled = scale_tokens(tokens_ref, gain_ref)
    first = jnp.dot(scaled, w1_ref[...], preferred_element_type=f32)
    second = jnp.dot(scaled, w2_ref[...], preferred_element_type=f32)
    value = jnp.dot(scaled, wv_ref[...], preferred_element_type=f32)
    for head in range(heads):
        columns = by_head(first, second, head)
        for group in range(scaled.shape[0] // ROWS):
            rows = slice(group * ROWS, (group + 1) * ROWS)
            at = slice(head * LANES, (head + 1) * LANES)
            out_ref[group * heads, :, at] = columns[rows].astype(bf16)
            out_ref[group * heads + 1, :, at] = value[rows, at].astype(bf16)


def finish_queries(heads, width, factor, part_ref, out_ref, inverse_ref):
    group = lax.axis_index("kv") // heads
    total = part_ref[0]
    for source in range(1, part_ref.shape[0]):
        total = total + part_ref[source]
    inverse = lax.rsqrt(total[:, ROWS * LANES :] / width + epsilon)
    tile = (ROWS, LANES)
    mine = lane_iota(tile) == group * ROWS + row_iota(tile)
    column = jnp.sum(jnp.where(mine, inverse, 0.0), axis=1, keepdims=True)
    sums = jnp.concatenate(
        [total[:, row * LANES : (row + 1) * LANES] for row in range(ROWS)], axis=0
    )
    query = (sums * column * factor).astype(bf16)
    inverse_ref[...] = jnp.broadcast_to(column, tile)
    for owner in range(out_ref.shape[0]):
        out_ref[owner] = query


def finish_values(part_ref, inverse_ref, out_ref):
    total = part_ref[0].astype(f32)
    for source in range(1, part_ref.shape[0]):
        total = total + part_ref[source].astype(f32)
    column = inverse_ref[:, 0:1]
    fresh = (total * column).astype(bf16)
    for owner in range(out_ref.shape[0]):
        out_ref[owner] = fresh


def two_maps(query):
    low = lane_iota(query.shape) < LANES // 2
    zero = jnp.zeros_like(query)
    return jnp.concatenate(
        [jnp.where(low, query, zero), jnp.where(low, zero, query)], axis=0
    ).astype(bf16)


def softmax_block(scores, visible):
    scores = jnp.where(visible, scores, masked_fill)
    maxima = jnp.max(scores, axis=1, keepdims=True)
    weights = jnp.where(visible, jnp.exp(scores - maxima), 0.0)
    return maxima, jnp.sum(weights, axis=1, keepdims=True), weights.astype(bf16)


def contract_last(left, right):
    return lax.dot_general(left, right, (((1,), (1,)), ((), ())), preferred_element_type=f32)


def in_pieces(value):
    high = value.astype(bf16).astype(f32)
    rest = value - high
    middle = rest.astype(bf16).astype(f32)
    return (high, middle, rest - middle)


PIECES = 6


def attend_cache(heads, query_ref, keys_ref, values_ref, lengths_ref, accepted_ref, out_ref):
    seqs, context = keys_ref.shape[1], keys_ref.shape[2]
    start = lax.axis_index("kv") * context
    for seq in range(seqs):
        limit = lengths_ref[seq] + accepted_ref[seq] - start
        for head in range(heads):
            owners = [(2 * seq + half) * heads + head for half in range(2)]
            query = jnp.concatenate([query_ref[o].astype(f32) for o in owners], axis=0)
            both = two_maps(query)
            scores = contract_last(both, keys_ref[head, seq])
            visible = lane_iota(scores.shape) < limit
            maxima, totals, weights = softmax_block(scores, visible)
            summed = jnp.dot(weights, values_ref[head, seq], preferred_element_type=f32)
            dims = summed.shape
            count = dims[0] // 2
            at = lane_iota(dims) - jnp.where(row_iota(dims) >= count, PIECES, 0)
            stats = jnp.zeros(dims, f32)
            for k, piece in enumerate(in_pieces(maxima) + in_pieces(totals)):
                stats = jnp.where(at == k, piece, stats)
            for half, owner in enumerate(owners):
                low, high = half * ROWS, count + half * ROWS
                first, second = slice(low, low + ROWS), slice(high, high + ROWS)
                out_ref[owner, :, 0:LANES] = summed[first].astype(bf16)
                out_ref[owner, :, LANES : 2 * LANES] = summed[second].astype(bf16)
                out_ref[owner, :, 2 * LANES :] = (stats[first] + stats[second]).astype(bf16)


def attend_tree(heads, query_ref, fresh_ref, parents_ref, out_ref, seen_ref):
    me = lax.axis_index("kv")
    head, group = lax.rem(me, heads), me // heads
    seq, half = group // 2, lax.rem(group, 2)
    nodes = parents_ref.shape[1]
    for node in range(nodes):
        parent = parents_ref[seq, node]
        above = jnp.where(parent >= 0, seen_ref[jnp.maximum(parent, 0)], 0) if node else 0
        seen_ref[node] = above | (1 << node)

    def rows_of(kind):
        tiles = []
        for part in range(2):
            both = fresh_ref[(2 * seq + part) * heads + kind].astype(f32)
            tiles.append(jnp.where(head == 0, both[:, :LANES], both[:, LANES:]))
        tiles.append(jnp.zeros((LANES - nodes, LANES), f32))
        return jnp.concatenate(tiles, axis=0).astype(bf16)

    both = two_maps(query_ref[0].astype(f32))
    scores = contract_last(both, rows_of(0))
    dims = scores.shape
    row = lax.rem(row_iota(dims), ROWS)
    bits = jnp.zeros(dims, jnp.int32)
    for k in range(ROWS):
        bits = jnp.where(row == k, seen_ref[half * ROWS + k], bits)
    lane = lane_iota(dims)
    visible = (lane < nodes) & ((lax.shift_right_logical(bits, jnp.minimum(lane, 31)) & 1) == 1)
    maxima, totals, weights = softmax_block(scores, visible)
    out_ref[0] = jnp.broadcast_to(maxima, dims)
    out_ref[1] = jnp.broadcast_to(totals, dims)
    out_ref[2] = jnp.dot(weights, rows_of(1), preferred_element_type=f32)


def join_blocks(heads, part_ref, tree_ref, lambdas_ref, gain_ref, out_ref):
    sources = part_ref.shape[0]
    head = lax.rem(lax.axis_index("kv"), heads)
    tile = (ROWS, LANES)
    pieces = jnp.concatenate(
        [part_ref[k][:, 2 * LANES :].astype(f32) for k in range(sources)], axis=0
    ).astype(bf16)
    pick_dims = (LANES, 4 * LANES)
    pick = jnp.where(row_iota(pick_dims) // 3 == lane_iota(pick_dims) // LANES, 1.0, 0.0)
    stats = jnp.dot(pieces, pick.astype(bf16), preferred_element_type=f32)
    attention = []
    for which in range(2):
        rows = slice(which * ROWS, (which + 1) * ROWS)
        low = 2 * which * LANES
        maxima = [stats[k * ROWS : (k + 1) * ROWS, low : low + LANES] for k in range(sources)]
        tree_max = tree_ref[0][rows]
        highest = tree_max
        for k in range(sources):
            highest = jnp.maximum(highest, maxima[k])
        scale = jnp.exp(tree_max - highest)
        totals = scale * tree_ref[1][rows]
        summed = scale * tree_ref[2][rows]
        for k in range(sources):
            factor = jnp.exp(maxima[k] - highest)
            total = stats[k * ROWS : (k + 1) * ROWS, low + LANES : low + 2 * LANES]
            totals = totals + factor * total
            block = part_ref[k][:, which * LANES : (which + 1) * LANES].astype(f32)
            summed = summed + factor * block
        attention.append(summed / totals)
    differ = attention[0] - lambdas_ref[head] * attention[1]
    mean = jnp.mean(differ * differ, axis=1, keepdims=True)
    normed = differ * lax.rsqrt(mean + epsilon)
    normed = (normed * gain_ref[...].astype(f32) * head_factor).astype(bf16)
    for owner in range(out_ref.shape[0]):
        out_ref[owner] = normed


def project_out(heads, head_out_ref, weight_ref, out_ref):
    groups = head_out_ref.shape[0] // heads
    total = None
    for head in range(heads):
        rows = jnp.concatenate(
            [head_out_ref[group * heads + head].astype(f32) for group in range(groups)], axis=0
        ).astype(bf16)
        weight = weight_ref[head * LANES : (head + 1) * LANES, :]
        term = jnp.dot(rows, weight, preferred_element_type=f32)
        total = term if total is None else total + term
    out_ref[...] = total.astype(bf16)


def add_groups(part_ref, out_ref):
    total = part_ref[0].astype(f32)
    for source in range(1, part_ref.shape[0]):
        total = total + part_ref[source].astype(f32)
    out_ref[...] = total.astype(bf16)


def exchange(pieces, axis):
    return lax.all_to_all(pieces, axis, split_axis=0, concat_axis=0, tiled=True)


def per_device(
    tokens,
    norm_gain,
    w_query1,
    w_query2,
    w_key1,
    w_key2,
    w_value,
    head_gain,
    lambdas,
    w_out,
    cache_keys,
    cache_values,
    lengths,
    accepted,
    parents,
):
    shards = lax.axis_size("kv")
    heads = cache_keys.shape[2]
    context = cache_keys.shape[1]
    seqs, nodes = parents.shape
    token_count = tokens.shape[0]
    qk_size = w_query1.shape[1] // heads
    width = tokens.shape[1] * shards
    assert token_count * heads == shards * ROWS and heads == 2 and nodes == 2 * ROWS
    assert 2 * qk_size == LANES and cache_values.shape[3] == LANES
    gain = norm_gain.reshape(1, -1)

    query_sent = call(
        functools.partial(query_parts, heads),
        shape((shards, 1, (ROWS + 1) * LANES), f32),
        [VMEM] * 4,
        "query_parts",
        2 * token_count * tokens.shape[1] * 2 * LANES,
    )(tokens, gain, w_query1, w_query2)
    query_got = exchange(query_sent, "kv")
    value_sent = call(
        functools.partial(value_parts, heads),
        shape((shards, ROWS, 2 * LANES), bf16),
        [VMEM] * 5,
        "value_parts",
        2 * token_count * tokens.shape[1] * 4 * LANES,
    )(tokens, gain, w_key1, w_key2, w_value)
    value_got = exchange(value_sent, "kv")
    keys_by_head = jnp.transpose(cache_keys, (2, 0, 1, 3))
    values_by_head = jnp.transpose(cache_values, (2, 0, 1, 3))

    query_mine, inverse = call(
        functools.partial(finish_queries, heads, width, qk_size ** (-0.5)),
        (shape((shards, ROWS, LANES), bf16), shape((ROWS, LANES), f32)),
        [VMEM],
        "finish_queries",
        1 << 20,
        out_specs=(VMEM, VMEM),
    )(query_got)
    queries = exchange(query_mine, "kv")
    fresh_mine = call(
        finish_values,
        shape((shards, ROWS, 2 * LANES), bf16),
        [VMEM, VMEM],
        "finish_values",
        1 << 20,
    )(value_got, inverse)
    fresh = exchange(fresh_mine, "kv")

    parts = call(
        functools.partial(attend_cache, heads),
        shape((shards, ROWS, 3 * LANES), bf16),
        [VMEM, VMEM, VMEM, SMEM, SMEM],
        "attend_cache",
        4 * token_count * 2 * heads * context * LANES,
    )(queries, keys_by_head, values_by_head, lengths, accepted)
    parts_got = exchange(parts, "kv")
    tree = call(
        functools.partial(attend_tree, heads),
        shape((3, 2 * ROWS, LANES), f32),
        [VMEM, VMEM, SMEM],
        "attend_tree",
        1 << 20,
        scratch=[pltpu.SMEM((nodes,), jnp.int32)],
    )(query_mine, fresh, parents)
    head_mine = call(
        functools.partial(join_blocks, heads),
        shape((shards, ROWS, LANES), bf16),
        [VMEM, VMEM, SMEM, VMEM],
        "join_blocks",
        1 << 22,
    )(parts_got, tree, lambdas, head_gain.reshape(1, -1))
    head_out = exchange(head_mine, "kv")
    product = call(
        functools.partial(project_out, heads),
        shape((token_count, w_out.shape[1]), bf16),
        [VMEM, VMEM],
        "project_out",
        2 * token_count * w_out.shape[0] * w_out.shape[1],
    )(head_out, w_out)
    groups = lax.axis_size("tp")
    product_got = exchange(product.reshape(groups, token_count // groups, -1), "tp")
    mixed = call(
        add_groups,
        shape((token_count // groups, w_out.shape[1]), bf16),
        [VMEM],
        "add_groups",
        1 << 20,
    )(product_got)

    by_kind = fresh.reshape(token_count // ROWS, 2, ROWS, heads, LANES)
    by_kind = jnp.moveaxis(by_kind, 1, 0).reshape(2, seqs, nodes, heads, LANES)
    valid_len = lengths + accepted
    positions = lax.axis_index("kv") * context + jnp.arange(context, dtype=jnp.int32)
    offsets = positions[None, :] - valid_len[:, None]
    picker = (offsets[:, :, None] == jnp.arange(nodes, dtype=jnp.int32)).astype(bf16)
    landed = ((offsets >= 0) & (offsets < nodes))[:, :, None, None]

    def write(cache, rows):
        placed = jnp.einsum("scp,sphd->schd", picker, rows, preferred_element_type=f32)
        return jnp.where(landed, placed.astype(bf16), cache)

    return mixed, write(cache_keys, by_kind[0]), write(cache_values, by_kind[1])


def solution(mesh):
    return jax.shard_map(
        per_device,
        mesh=mesh,
        in_specs=(
            P("grp", "kv"),
            P("kv"),
            P("kv", "tp"),
            P("kv", "tp"),
            P("kv", "tp"),
            P("kv", "tp"),
            P("kv", "tp"),
            P(),
            P("tp"),
            P("tp", "kv"),
            P("grp", "kv", "tp", None),
            P("grp", "kv", "tp", None),
            P("grp"),
            P("grp"),
            P("grp", None),
        ),
        out_specs=(P(("grp", "tp"), "kv"), P("grp", "kv", "tp", None), P("grp", "kv", "tp", None)),
        check_vma=False,
    )
```

time: 262 us -> 260 us (level)
  blocking collectives: 104 us -> 0 us
  starting transfers between devices: 27.8 us -> 85.4 us
  waiting for transfers between devices: 96.8 us -> 142 us
  Pallas kernels: 0 us -> 20 us
  matrix products: 11.2 us -> 1.64 us
  local copies, waits for them, and re-layouts: 14.5 us -> 9.09 us
  other arithmetic: 4.97 us -> 0.15 us
    all_to_all x1 -> x0, blocking collectives: 104 us -> none  [sum_at_owner(): lax.all_to_all(split_up(shard, dim, devices), axis, 0, 0, tiled=True)]
    all_to_all x4 -> x7, starting transfers between devices: 27.8 us -> 85.4 us  [exchange(): return lax.all_to_all(pieces, axis, split_axis=0, concat_axis=0, tiled=True)]
    all_to_all x4 -> x7, waiting for transfers between devices: 96.8 us -> 142 us  [exchange(): return lax.all_to_all(pieces, axis, split_axis=0, concat_axis=0, tiled=True)]
    pallas_call x0 -> x9, Pallas kernels: none -> 20 us  [the longest x1 6.16 us: per_device(): call(functools.partial(attend_cache, heads), shape((shards, ROWS, 3 * LAN...]
    dot_general x19 -> x2, matrix products: 11.2 us -> 1.64 us  [write(): jnp.einsum('scp,sphd->schd', picker, rows, preferred_element_type=f32)]
    reduce_sum x9 -> x0, other arithmetic: 3.1 us -> none  [the longest x1 0.86 us: per_device(): squares = jnp.sum(wide_tokens * wide_tokens, axis=1)]
    transpose x4 -> x1, local copies, waits for them, and re-layouts: 0.06 us -> 3.02 us  [per_device(): values_by_head = jnp.transpose(cache_values, (2, 0, 1, 3))]
    unnamed x36 -> x24, local copies, waits for them, and re-layouts: 4.99 us -> 6.04 us
  transfers between devices with their start and end apart: 4 -> 7, of which waited for: 3 -> 6; matrix products, arithmetic and copies ran while one was open for 4% -> 3% of each run, Pallas kernels for 0% -> 5%
where the time goes in v1:
time: 260 us; the launch traced here: 259 us
  waiting for transfers between devices  142 us (55%)
  starting transfers between devices  85.4 us (33%)
  Pallas kernels  20 us (8%)
  local copies, waits for them, and re-layouts  9.09 us (3%)
    all_to_all x7, waiting for transfers between devices, exchange(): return lax.all_to_all(pieces, axis, split_axis=0, concat_axis=0, tiled=True)  142 us
    all_to_all x7, starting transfers between devices, exchange(): return lax.all_to_all(pieces, axis, split_axis=0, concat_axis=0, tiled=True)  85.4 us
    pallas_call x1, Pallas kernels, per_device(): call(functools.partial(attend_cache, heads), shape((shards, ROWS, 3 * LAN...  6.16 us
    unnamed x24, local copies, waits for them, and re-layouts  6.04 us
  transfers between devices with their start and end apart: 7, of which 6 were waited for; matrix products, arithmetic and copies ran while one was open for 3% of the time, Pallas kernels for 5%

profile of v1, /device:TPU:33, one launch (start us, length us, event | category | flops | bytes accessed | tf_op | source)
XLA Modules:
  0.0 258.9 jit_solution(13643501818172965093)
XLA Ops:
  0.6 0.0 copy-start.1
  0.6 1.8 query_parts.1
  2.5 46.3 %all-to-all-start = ((f32[32,1,1152]{2,1,0:T(1,128)}), f32[32,1,1152]{2,1,0:T(1,128)S(1)}, u32[]{:S(2)}, u32[]{:S(2)}) async-start(f32[32,1,1152]{2,1,0:T(1,128)} %query_parts.1), calls=%async_computation | async-start | bytes 294912 | tf_op jit(solution)/shard_map/all_to_all | solution.py:262
  48.8 1.8 value_parts.1
  50.6 28.9 %all-to-all-done.part_ref = f32[32,1,1152]{2,1,0:T(1,128)S(1)} async-done(((f32[32,1,1152]{2,1,0:T(1,128)}), f32[32,1,1152]{2,1,0:T(1,128)S(1)}, u32[]{:S(2)}, u32[]{:S(2)}) %all-to-all-start) | async-done | bytes 147488 | tf_op jit(solution)/shard_map/all_to_all | solution.py:262
  79.5 0.0 copy-start.4
  79.5 4.8 %all-to-all-start.3 = ((bf16[32,8,256]{2,1,0:T(8,128)(2,1)}), bf16[32,8,256]{2,1,0:T(8,128)(2,1)S(1)}, u32[]{:S(2)}, u32[]{:S(2)}) async-start(bf16[32,8,256]{2,1,0:T(8,128)(2,1)} %value_parts.1), calls=%async_computation.3 | async-start | bytes 262144 | tf_op jit(solution)/shard_map/all_to_all | solution.py:262
  84.3 0.0 copy-done.4
  84.3 1.7 finish_queries.1
  85.9 25.1 %all-to-all-done.3.part_ref = bf16[32,8,256]{2,1,0:T(8,128)(2,1)S(1)} async-done(((bf16[32,8,256]{2,1,0:T(8,128)(2,1)}), bf16[32,8,256]{2,1,0:T(8,128)(2,1)S(1)}, u32[]{:S(2)}, u32[]{:S(2)}) %all-to-all-start.3) | async-done | bytes 131104 | tf_op jit(solution)/shard_map/all_to_all | solution.py:262
  111.1 0.0 copy-start.5
  111.1 6.4 %all-to-all-start.1 = ((bf16[32,8,128]{2,1,0:T(8,128)(2,1)}), bf16[32,8,128]{2,1,0:T(8,128)(2,1)S(1)}, u32[]{:S(2)}, u32[]{:S(2)}) async-start(bf16[32,8,128]{2,1,0:T(8,128)(2,1)} %get-tuple-element.5.query_ref), calls=%async_computation.1 | async-start | bytes 131072 | tf_op jit(solution)/shard_map/all_to_all | solution.py:262
  117.5 0.0 copy-done.5
  117.5 1.6 finish_values.1
  119.1 21.1 %all-to-all-done.1.query_ref = bf16[32,8,128]{2,1,0:T(8,128)(2,1)S(1)} async-done(((bf16[32,8,128]{2,1,0:T(8,128)(2,1)}), bf16[32,8,128]{2,1,0:T(8,128)(2,1)S(1)}, u32[]{:S(2)}, u32[]{:S(2)}) %all-to-all-start.1) | async-done | bytes 65568 | tf_op jit(solution)/shard_map/all_to_all | solution.py:262
  140.2 0.0 copy-start.6
  140.2 4.7 %all-to-all-start.4 = ((bf16[32,8,256]{2,1,0:T(8,128)(2,1)}), bf16[32,8,256]{2,1,0:T(8,128)(2,1)S(1)}, u32[]{:S(2)}, u32[]{:S(2)}) async-start(bf16[32,8,256]{2,1,0:T(8,128)(2,1)} %finish_values.1), calls=%async_computation.4 | async-start | bytes 262144 | tf_op jit(solution)/shard_map/all_to_all | solution.py:262
  145.0 0.0 copy-done.1
  145.0 3.0 %copy_bitcast_fusion = (bf16[2,8,256,128]{3,2,1,0:T(8,128)(2,1)}, bf16[2,8,256,128]{3,2,1,0:T(8,128)(2,1)}) fusion(bf16[8,256,2,128]{3,2,1,0:T(2,128)(2,1)} %param.26, bf16[8,256,2,128]{3,2,1,0:T(2,128)(2,1)S(1)} %copy-done.1), kind=kLoop, calls=%fused_computation.4 | loop fusion | bytes 4194304 | tf_op jit(solution)/shard_map/transpose | solution.py:310
  148.0 0.0 copy-done.6
  148.0 0.0 copy-start.9
  148.0 0.0 copy-start.10
  148.0 6.2 %attend_cache.1 = bf16[32,8,384]{2,1,0:T(8,128)(2,1)} custom-call(bf16[32,8,128]{2,1,0:T(8,128)(2,1)} %copy-done.6, bf16[2,8,256,128]{3,2,1,0:T(8,128)(2,1)} %get-tuple-element.16.keys_ref, bf16[2,8,256,128]{3,2,1,0:T(8,128)(2,1)} %get-tuple-element.15.values_ref, s32[8]{0:T(128)} %lengths_ref.1, s32[8]{0:T(128)} %accepted_ref.1), custom_call_target="tpu_custom_call" | custom-call | flops 67108864 | bytes 65536 | tf_op jit(solution)/shard_map/attend_cache/pallas_call | solution.py:330
  154.2 16.7 %all-to-all-done.4.fresh_ref = bf16[32,8,256]{2,1,0:T(8,128)(2,1)S(1)} async-done(((bf16[32,8,256]{2,1,0:T(8,128)(2,1)}), bf16[32,8,256]{2,1,0:T(8,128)(2,1)S(1)}, u32[]{:S(2)}, u32[]{:S(2)}) %all-to-all-start.4) | async-done | bytes 131104 | tf_op jit(solution)/shard_map/all_to_all | solution.py:262
  170.8 5.7 %all-to-all-start.2 = ((bf16[32,8,384]{2,1,0:T(8,128)(2,1)}), bf16[32,8,384]{2,1,0:T(8,128)(2,1)S(1)}, u32[]{:S(2)}, u32[]{:S(2)}) async-start(bf16[32,8,384]{2,1,0:T(8,128)(2,1)} %attend_cache.1), calls=%async_computation.2 | async-start | bytes 393216 | tf_op jit(solution)/shard_map/all_to_all | solution.py:262
  176.6 0.0 copy-done.9
  176.6 0.0 copy-done.10
  176.6 0.1 compare_and_fusion
  176.7 0.1 broadcast_subtract_fusion
  176.8 0.0 copy-done
  176.8 1.9 attend_tree.1.tree_ref
  178.7 28.2 %all-to-all-done.2.part_ref = bf16[32,8,384]{2,1,0:T(8,128)(2,1)S(1)} async-done(((bf16[32,8,384]{2,1,0:T(8,128)(2,1)}), bf16[32,8,384]{2,1,0:T(8,128)(2,1)S(1)}, u32[]{:S(2)}, u32[]{:S(2)}) %all-to-all-start.2) | async-done | bytes 196640 | tf_op jit(solution)/shard_map/all_to_all | solution.py:262
  206.9 0.7 copy-done.3
  207.6 2.0 join_blocks.1
  209.6 7.3 %all-to-all-start.5 = ((bf16[32,8,128]{2,1,0:T(8,128)(2,1)}), bf16[32,8,128]{2,1,0:T(8,128)(2,1)S(1)}, u32[]{:S(2)}, u32[]{:S(2)}) async-start(bf16[32,8,128]{2,1,0:T(8,128)(2,1)} %join_blocks.1), calls=%async_computation.5 | async-start | bytes 131072 | tf_op jit(solution)/shard_map/all_to_all | solution.py:262
  216.9 0.0 copy-start.2
  216.9 0.8 fusion
  217.7 21.8 %all-to-all-done.5.head_out_ref = bf16[32,8,128]{2,1,0:T(8,128)(2,1)S(1)} async-done(((bf16[32,8,128]{2,1,0:T(8,128)(2,1)}), bf16[32,8,128]{2,1,0:T(8,128)(2,1)S(1)}, u32[]{:S(2)}, u32[]{:S(2)}) %all-to-all-start.5) | async-done | bytes 65568 | tf_op jit(solution)/shard_map/all_to_all | solution.py:262
  239.6 0.6 copy-done.7
  240.2 1.6 project_out.1
  241.8 10.2 %all-to-all-start.6 = ((bf16[8,16,128]{2,1,0:T(8,128)(2,1)}), bf16[8,16,128]{2,1,0:T(8,128)(2,1)S(1)}, u32[]{:S(2)}, u32[]{:S(2)}) async-start(bf16[8,16,128]{2,1,0:T(8,128)(2,1)} %bitcast.21), calls=%async_computation.6 | async-start | bytes 65536 | tf_op jit(solution)/shard_map/all_to_all | solution.py:262
  252.0 0.0 copy-done.2
  252.0 0.8 fusion.1
  252.8 2.0 copy.31
  254.9 2.0 copy.32
  256.9 0.0 all-to-all-done.6.part_ref
  256.9 0.6 copy-done.8
  257.5 1.4 add_groups.1
  (8 shorter events, 0.0 us)
Async XLA Ops:
  0.6 144.3 %copy-start.1 = (bf16[8,256,2,128]{3,2,1,0:T(2,128)(2,1)S(1)}, bf16[8,256,2,128]{3,2,1,0:T(2,128)(2,1)}, u32[]{:S(2)}) copy-start(bf16[8,256,2,128]{3,2,1,0:T(2,128)(2,1)} %param.25) | copy-start | bytes 3145732
  2.5 77.0 %all-to-all-start = ((f32[32,1,1152]{2,1,0:T(1,128)}), f32[32,1,1152]{2,1,0:T(1,128)S(1)}, u32[]{:S(2)}, u32[]{:S(2)}) async-start(f32[32,1,1152]{2,1,0:T(1,128)} %query_parts.1), calls=%async_computation | async-start | bytes 294912 | tf_op jit(solution)/shard_map/all_to_all | solution.py:262
  79.5 4.8 %copy-start.4 = (f32[32,1,1152]{2,1,0:T(1,128)}, f32[32,1,1152]{2,1,0:T(1,128)S(1)}, u32[]{:S(2)}) copy-start(f32[32,1,1152]{2,1,0:T(1,128)S(1)} %all-to-all-done.part_ref) | copy-start | bytes 442372
  79.5 31.6 %all-to-all-start.3 = ((bf16[32,8,256]{2,1,0:T(8,128)(2,1)}), bf16[32,8,256]{2,1,0:T(8,128)(2,1)S(1)}, u32[]{:S(2)}, u32[]{:S(2)}) async-start(bf16[32,8,256]{2,1,0:T(8,128)(2,1)} %value_parts.1), calls=%async_computation.3 | async-start | bytes 262144 | tf_op jit(solution)/shard_map/all_to_all | solution.py:262
  111.1 6.4 %copy-start.5 = (bf16[32,8,256]{2,1,0:T(8,128)(2,1)}, bf16[32,8,256]{2,1,0:T(8,128)(2,1)S(1)}, u32[]{:S(2)}) copy-start(bf16[32,8,256]{2,1,0:T(8,128)(2,1)S(1)} %all-to-all-done.3.part_ref) | copy-start | bytes 393220
  111.1 29.2 %all-to-all-start.1 = ((bf16[32,8,128]{2,1,0:T(8,128)(2,1)}), bf16[32,8,128]{2,1,0:T(8,128)(2,1)S(1)}, u32[]{:S(2)}, u32[]{:S(2)}) async-start(bf16[32,8,128]{2,1,0:T(8,128)(2,1)} %get-tuple-element.5.query_ref), calls=%async_computation.1 | async-start | bytes 131072 | tf_op jit(solution)/shard_map/all_to_all | solution.py:262
  140.2 7.8 %copy-start.6 = (bf16[32,8,128]{2,1,0:T(8,128)(2,1)}, bf16[32,8,128]{2,1,0:T(8,128)(2,1)S(1)}, u32[]{:S(2)}) copy-start(bf16[32,8,128]{2,1,0:T(8,128)(2,1)S(1)} %all-to-all-done.1.query_ref) | copy-start | bytes 196612
  140.2 30.6 %all-to-all-start.4 = ((bf16[32,8,256]{2,1,0:T(8,128)(2,1)}), bf16[32,8,256]{2,1,0:T(8,128)(2,1)S(1)}, u32[]{:S(2)}, u32[]{:S(2)}) async-start(bf16[32,8,256]{2,1,0:T(8,128)(2,1)} %finish_values.1), calls=%async_computation.4 | async-start | bytes 262144 | tf_op jit(solution)/shard_map/all_to_all | solution.py:262
  148.0 28.6 %copy-start.9 = (s32[8]{0:T(128)S(1)}, s32[8]{0:T(128)}, u32[]{:S(2)}) copy-start(s32[8]{0:T(128)} %lengths_ref.1) | copy-start | bytes 100
  148.0 28.6 %copy-start.10 = (s32[8]{0:T(128)S(1)}, s32[8]{0:T(128)}, u32[]{:S(2)}) copy-start(s32[8]{0:T(128)} %accepted_ref.1) | copy-start | bytes 100
  170.8 6.0 %copy-start = (bf16[32,8,256]{2,1,0:T(8,128)(2,1)}, bf16[32,8,256]{2,1,0:T(8,128)(2,1)S(1)}, u32[]{:S(2)}) copy-start(bf16[32,8,256]{2,1,0:T(8,128)(2,1)S(1)} %all-to-all-done.4.fresh_ref) | copy-start | bytes 393220
  170.8 36.1 %all-to-all-start.2 = ((bf16[32,8,384]{2,1,0:T(8,128)(2,1)}), bf16[32,8,384]{2,1,0:T(8,128)(2,1)S(1)}, u32[]{:S(2)}, u32[]{:S(2)}) async-start(bf16[32,8,384]{2,1,0:T(8,128)(2,1)} %attend_cache.1), calls=%async_computation.2 | async-start | bytes 393216 | tf_op jit(solution)/shard_map/all_to_all | solution.py:262
  206.9 0.7 copy-start.3
  209.6 30.0 %all-to-all-start.5 = ((bf16[32,8,128]{2,1,0:T(8,128)(2,1)}), bf16[32,8,128]{2,1,0:T(8,128)(2,1)S(1)}, u32[]{:S(2)}, u32[]{:S(2)}) async-start(bf16[32,8,128]{2,1,0:T(8,128)(2,1)} %join_blocks.1), calls=%async_computation.5 | async-start | bytes 131072 | tf_op jit(solution)/shard_map/all_to_all | solution.py:262
  216.9 35.1 %copy-start.2 = (bf16[8,256,2,128]{3,2,1,0:T(2,128)(2,1)S(1)}, bf16[8,256,2,128]{3,2,1,0:T(2,128)(2,1)}, u32[]{:S(2)}) copy-start(bf16[8,256,2,128]{3,2,1,0:T(2,128)(2,1)} %param.26) | copy-start | bytes 3145732
  239.5 0.6 copy-start.7
  241.8 15.1 %all-to-all-start.6 = ((bf16[8,16,128]{2,1,0:T(8,128)(2,1)}), bf16[8,16,128]{2,1,0:T(8,128)(2,1)S(1)}, u32[]{:S(2)}, u32[]{:S(2)}) async-start(bf16[8,16,128]{2,1,0:T(8,128)(2,1)} %bitcast.21), calls=%async_computation.6 | async-start | bytes 65536 | tf_op jit(solution)/shard_map/all_to_all | solution.py:262
  256.9 0.6 copy-start.8

commit v2 on v1

--- a/solution.py
+++ b/solution.py
@@ -12,6 +12,9 @@
 head_factor = 0.8
 LANES = 128
 ROWS = 8
+HALF = ROWS // 2
+PIECES = 6
+VMEM_BYTES = 16 << 20
 
 f32 = jnp.float32
 bf16 = jnp.bfloat16
@@ -26,6 +29,7 @@
         in_specs=in_specs,
         out_specs=out_specs,
         scratch_shapes=scratch,
+        compiler_params=pltpu.CompilerParams(vmem_limit_bytes=VMEM_BYTES),
         cost_estimate=pl.CostEstimate(flops=flops, bytes_accessed=1 << 16, transcendentals=0),
         name=name,
     )
@@ -55,61 +59,75 @@
     return jnp.concatenate([left, right], axis=1)
 
 
-def query_parts(heads, tokens_ref, gain_ref, w1_ref, w2_ref, out_ref):
+def in_pieces(value):
+    high = value.astype(bf16).astype(f32)
+    rest = value - high
+    middle = rest.astype(bf16).astype(f32)
+    return (high, middle, rest - middle)
+
+
+def put_halves(out_ref, owner, at, tile):
+    for half in range(2):
+        lanes = slice((at + half) * LANES, (at + half + 1) * LANES)
+        out_ref[owner, :, lanes] = tile[half * HALF : (half + 1) * HALF].astype(bf16)
+
+
+def take_halves(value, at):
+    low, high = at * LANES, (at + 1) * LANES
+    return jnp.concatenate([value[:, low:high], value[:, high : high + LANES]], axis=0)
+
+
+def projection_parts(
+    heads, tokens_ref, gain_ref, q1_ref, q2_ref, k1_ref, k2_ref, v_ref, out_ref
+):
     wide, scaled = scale_tokens(tokens_ref, gain_ref)
-    first = jnp.dot(scaled, w1_ref[...], preferred_element_type=f32)
-    second = jnp.dot(scaled, w2_ref[...], preferred_element_type=f32)
-    squares = jnp.sum(jnp.transpose(wide * wide), axis=0, keepdims=True)
-    for head in range(heads):
-        columns = by_head(first, second, head)
-        for group in range(wide.shape[0] // ROWS):
+    first, second, key1, key2, value = [
+        jnp.dot(scaled, ref[...], preferred_element_type=f32)
+        for ref in (q1_ref, q2_ref, k1_ref, k2_ref, v_ref)
+    ]
+    dims = wide.shape
+    squares = in_pieces(jnp.sum(wide * wide, axis=1, keepdims=True))
+    at = lane_iota(dims) - jnp.where(lax.rem(row_iota(dims), ROWS) >= HALF, 3, 0)
+    stats = jnp.zeros(dims, f32)
+    for k, piece in enumerate(squares):
+        stats = jnp.where(at == k, piece, stats)
+    queries = [by_head(first, second, head) for head in range(heads)]
+    highs = [query.astype(bf16).astype(f32) for query in queries]
+    lows = [query - high for query, high in zip(queries, highs)]
+    keys = [by_head(key1, key2, head) for head in range(heads)]
+    values = [value[:, head * LANES : (head + 1) * LANES] for head in range(heads)]
+    for group in range(dims[0] // ROWS):
+        rows = slice(group * ROWS, (group + 1) * ROWS)
+        tile = stats[rows]
+        packed = tile[:HALF] + tile[HALF:]
+        for head in range(heads):
             owner = group * heads + head
-            for row in range(ROWS):
-                at = group * ROWS + row
-                out_ref[owner, :, row * LANES : (row + 1) * LANES] = columns[at : at + 1, :]
-            out_ref[owner, :, ROWS * LANES :] = squares
-
-
-def value_parts(heads, tokens_ref, gain_ref, w1_ref, w2_ref, wv_ref, out_ref):
-    _, scaled = scale_tokens(tokens_ref, gain_ref)
-    first = jnp.dot(scaled, w1_ref[...], preferred_element_type=f32)
-    second = jnp.dot(scaled, w2_ref[...], preferred_element_type=f32)
-    value = jnp.dot(scaled, wv_ref[...], preferred_element_type=f32)
-    for head in range(heads):
-        columns = by_head(first, second, head)
-        for group in range(scaled.shape[0] // ROWS):
-            rows = slice(group * ROWS, (group + 1) * ROWS)
-            at = slice(head * LANES, (head + 1) * LANES)
-            out_ref[group * heads, :, at] = columns[rows].astype(bf16)
-            out_ref[group * heads + 1, :, at] = value[rows, at].astype(bf16)
-
-
-def finish_queries(heads, width, factor, part_ref, out_ref, inverse_ref):
-    group = lax.axis_index("kv") // heads
-    total = part_ref[0]
-    for source in range(1, part_ref.shape[0]):
-        total = total + part_ref[source]
-    inverse = lax.rsqrt(total[:, ROWS * LANES :] / width + epsilon)
-    tile = (ROWS, LANES)
-    mine = lane_iota(tile) == group * ROWS + row_iota(tile)
-    column = jnp.sum(jnp.where(mine, inverse, 0.0), axis=1, keepdims=True)
-    sums = jnp.concatenate(
-        [total[:, row * LANES : (row + 1) * LANES] for row in range(ROWS)], axis=0
-    )
-    query = (sums * column * factor).astype(bf16)
-    inverse_ref[...] = jnp.broadcast_to(column, tile)
-    for owner in range(out_ref.shape[0]):
-        out_ref[owner] = query
-
-
-def finish_values(part_ref, inverse_ref, out_ref):
+            put_halves(out_ref, owner, 0, highs[head][rows])
+            put_halves(out_ref, owner, 2, lows[head][rows])
+            for column, array in enumerate((keys, values)[head]):
+                put_halves(out_ref, owner, 4 + 2 * column, array[rows])
+            out_ref[owner, :, 8 * LANES :] = packed.astype(bf16)
+
+
+def finish_projections(width, factor, part_ref, out_ref):
     total = part_ref[0].astype(f32)
     for source in range(1, part_ref.shape[0]):
         total = total + part_ref[source].astype(f32)
-    column = inverse_ref[:, 0:1]
-    fresh = (total * column).astype(bf16)
+    stats = total[:, 8 * LANES :]
+    lane = lane_iota(stats.shape)
+    squares = jnp.concatenate(
+        [
+            jnp.sum(jnp.where(lane // 3 == half, stats, 0.0), axis=1, keepdims=True)
+            for half in range(2)
+        ],
+        axis=0,
+    )
+    inverse = lax.rsqrt(squares / width + epsilon)
+    query = (take_halves(total, 0) + take_halves(total, 2)) * inverse * factor
+    fresh = [take_halves(total, at) * inverse for at in (4, 6)]
+    mine = jnp.concatenate([query] + fresh, axis=1).astype(bf16)
     for owner in range(out_ref.shape[0]):
-        out_ref[owner] = fresh
+        out_ref[owner] = mine
 
 
 def two_maps(query):
@@ -129,16 +147,6 @@
 
 def contract_last(left, right):
     return lax.dot_general(left, right, (((1,), (1,)), ((), ())), preferred_element_type=f32)
-
-
-def in_pieces(value):
-    high = value.astype(bf16).astype(f32)
-    rest = value - high
-    middle = rest.astype(bf16).astype(f32)
-    return (high, middle, rest - middle)
-
-
-PIECES = 6
 
 
 def attend_cache(heads, query_ref, keys_ref, values_ref, lengths_ref, accepted_ref, out_ref):
@@ -148,7 +156,7 @@
         limit = lengths_ref[seq] + accepted_ref[seq] - start
         for head in range(heads):
             owners = [(2 * seq + half) * heads + head for half in range(2)]
-            query = jnp.concatenate([query_ref[o].astype(f32) for o in owners], axis=0)
+            query = jnp.concatenate([query_ref[o][:, :LANES].astype(f32) for o in owners], axis=0)
             both = two_maps(query)
             scores = contract_last(both, keys_ref[head, seq])
             visible = lane_iota(scores.shape) < limit
@@ -156,19 +164,22 @@
             summed = jnp.dot(weights, values_ref[head, seq], preferred_element_type=f32)
             dims = summed.shape
             count = dims[0] // 2
-            at = lane_iota(dims) - jnp.where(row_iota(dims) >= count, PIECES, 0)
+            row = row_iota(dims)
+            at = lane_iota(dims) - jnp.where(row >= count, PIECES, 0)
+            at = at - jnp.where(lax.rem(row, ROWS) >= HALF, 2 * PIECES, 0)
             stats = jnp.zeros(dims, f32)
             for k, piece in enumerate(in_pieces(maxima) + in_pieces(totals)):
                 stats = jnp.where(at == k, piece, stats)
             for half, owner in enumerate(owners):
                 low, high = half * ROWS, count + half * ROWS
                 first, second = slice(low, low + ROWS), slice(high, high + ROWS)
-                out_ref[owner, :, 0:LANES] = summed[first].astype(bf16)
-                out_ref[owner, :, LANES : 2 * LANES] = summed[second].astype(bf16)
-                out_ref[owner, :, 2 * LANES :] = (stats[first] + stats[second]).astype(bf16)
-
-
-def attend_tree(heads, query_ref, fresh_ref, parents_ref, out_ref, seen_ref):
+                put_halves(out_ref, owner, 0, summed[first])
+                put_halves(out_ref, owner, 2, summed[second])
+                tile = stats[first] + stats[second]
+                out_ref[owner, :, 4 * LANES :] = (tile[:HALF] + tile[HALF:]).astype(bf16)
+
+
+def attend_tree(heads, mine_ref, fresh_ref, parents_ref, out_ref, seen_ref):
     me = lax.axis_index("kv")
     head, group = lax.rem(me, heads), me // heads
     seq, half = group // 2, lax.rem(group, 2)
@@ -182,11 +193,13 @@
         tiles = []
         for part in range(2):
             both = fresh_ref[(2 * seq + part) * heads + kind].astype(f32)
-            tiles.append(jnp.where(head == 0, both[:, :LANES], both[:, LANES:]))
+            tiles.append(
+                jnp.where(head == 0, both[:, LANES : 2 * LANES], both[:, 2 * LANES :])
+            )
         tiles.append(jnp.zeros((LANES - nodes, LANES), f32))
         return jnp.concatenate(tiles, axis=0).astype(bf16)
 
-    both = two_maps(query_ref[0].astype(f32))
+    both = two_maps(mine_ref[0][:, :LANES].astype(f32))
     scores = contract_last(both, rows_of(0))
     dims = scores.shape
     row = lax.rem(row_iota(dims), ROWS)
@@ -205,9 +218,11 @@
     sources = part_ref.shape[0]
     head = lax.rem(lax.axis_index("kv"), heads)
     tile = (ROWS, LANES)
-    pieces = jnp.concatenate(
-        [part_ref[k][:, 2 * LANES :].astype(f32) for k in range(sources)], axis=0
-    ).astype(bf16)
+    pieces = []
+    for k in range(sources):
+        packed = part_ref[k][:, 4 * LANES :].astype(f32)
+        pieces += [packed, pltpu.roll(packed, LANES - 2 * PIECES, 1)]
+    pieces = jnp.concatenate(pieces, axis=0).astype(bf16)
     pick_dims = (LANES, 4 * LANES)
     pick = jnp.where(row_iota(pick_dims) // 3 == lane_iota(pick_dims) // LANES, 1.0, 0.0)
     stats = jnp.dot(pieces, pick.astype(bf16), preferred_element_type=f32)
@@ -227,8 +242,8 @@
             factor = jnp.exp(maxima[k] - highest)
             total = stats[k * ROWS : (k + 1) * ROWS, low + LANES : low + 2 * LANES]
             totals = totals + factor * total
-            block = part_ref[k][:, which * LANES : (which + 1) * LANES].astype(f32)
-            summed = summed + factor * block
+            block = part_ref[k][:, 2 * which * LANES : 2 * (which + 1) * LANES].astype(f32)
+            summed = summed + factor * take_halves(block, 0)
         attention.append(summed / totals)
     differ = attention[0] - lambdas_ref[head] * attention[1]
     mean = jnp.mean(differ * differ, axis=1, keepdims=True)
@@ -290,50 +305,32 @@
     assert 2 * qk_size == LANES and cache_values.shape[3] == LANES
     gain = norm_gain.reshape(1, -1)
 
-    query_sent = call(
-        functools.partial(query_parts, heads),
-        shape((shards, 1, (ROWS + 1) * LANES), f32),
-        [VMEM] * 4,
-        "query_parts",
-        2 * token_count * tokens.shape[1] * 2 * LANES,
-    )(tokens, gain, w_query1, w_query2)
-    query_got = exchange(query_sent, "kv")
-    value_sent = call(
-        functools.partial(value_parts, heads),
-        shape((shards, ROWS, 2 * LANES), bf16),
-        [VMEM] * 5,
-        "value_parts",
-        2 * token_count * tokens.shape[1] * 4 * LANES,
-    )(tokens, gain, w_key1, w_key2, w_value)
-    value_got = exchange(value_sent, "kv")
+    sent = call(
+        functools.partial(projection_parts, heads),
+        shape((shards, HALF, 9 * LANES), bf16),
+        [VMEM] * 7,
+        "projection_parts",
+        2 * token_count * tokens.shape[1] * 6 * LANES,
+    )(tokens, gain, w_query1, w_query2, w_key1, w_key2, w_value)
+    got = exchange(sent, "kv")
     keys_by_head = jnp.transpose(cache_keys, (2, 0, 1, 3))
     values_by_head = jnp.transpose(cache_values, (2, 0, 1, 3))
-
-    query_mine, inverse = call(
-        functools.partial(finish_queries, heads, width, qk_size ** (-0.5)),
-        (shape((shards, ROWS, LANES), bf16), shape((ROWS, LANES), f32)),
+    mine = call(
+        functools.partial(finish_projections, width, qk_size ** (-0.5)),
+        shape((shards, ROWS, 3 * LANES), bf16),
         [VMEM],
-        "finish_queries",
+        "finish_projections",
         1 << 20,
-        out_specs=(VMEM, VMEM),
-    )(query_got)
-    queries = exchange(query_mine, "kv")
-    fresh_mine = call(
-        finish_values,
-        shape((shards, ROWS, 2 * LANES), bf16),
-        [VMEM, VMEM],
-        "finish_values",
-        1 << 20,
-    )(value_got, inverse)
-    fresh = exchange(fresh_mine, "kv")
+    )(got)
+    projected = exchange(mine, "kv")
 
     parts = call(
         functools.partial(attend_cache, heads),
-        shape((shards, ROWS, 3 * LANES), bf16),
+        shape((shards, HALF, 5 * LANES), bf16),
         [VMEM, VMEM, VMEM, SMEM, SMEM],
         "attend_cache",
         4 * token_count * 2 * heads * context * LANES,
-    )(queries, keys_by_head, values_by_head, lengths, accepted)
+    )(projected, keys_by_head, values_by_head, lengths, accepted)
     parts_got = exchange(parts, "kv")
     tree = call(
         functools.partial(attend_tree, heads),
@@ -342,7 +339,7 @@
         "attend_tree",
         1 << 20,
         scratch=[pltpu.SMEM((nodes,), jnp.int32)],
-    )(query_mine, fresh, parents)
+    )(mine, projected, parents)
     head_mine = call(
         functools.partial(join_blocks, heads),
         shape((shards, ROWS, LANES), bf16),
@@ -368,7 +365,7 @@
         1 << 20,
     )(product_got)
 
-    by_kind = fresh.reshape(token_count // ROWS, 2, ROWS, heads, LANES)
+    by_kind = projected[:, :, LANES:].reshape(token_count // ROWS, 2, ROWS, heads, LANES)
     by_kind = jnp.moveaxis(by_kind, 1, 0).reshape(2, seqs, nodes, heads, LANES)
     valid_len = lengths + accepted
     positions = lax.axis_index("kv") * context + jnp.arange(context, dtype=jnp.int32)

time: 260 us -> 222 us (0.85)
  blocking collectives: 0 us -> 90 us
  waiting for transfers between devices: 142 us -> 80.7 us
  starting transfers between devices: 85.4 us -> 26.2 us
  Pallas kernels: 20 us -> 10.6 us
    all_to_all x0 -> x1, blocking collectives: none -> 90 us  [exchange(): return lax.all_to_all(pieces, axis, split_axis=0, concat_axis=0, tiled=True)]
    all_to_all x7 -> x4, waiting for transfers between devices: 142 us -> 80.7 us  [exchange(): return lax.all_to_all(pieces, axis, split_axis=0, concat_axis=0, tiled=True)]
    all_to_all x7 -> x4, starting transfers between devices: 85.4 us -> 26.2 us  [exchange(): return lax.all_to_all(pieces, axis, split_axis=0, concat_axis=0, tiled=True)]
    pallas_call x5 -> x3, Pallas kernels: 13.1 us -> 6.27 us  [the longest x1 5.1 us: per_device(): call(functools.partial(attend_cache, heads), shape((shards, HALF, 5 * LAN...]
    unnamed x24 -> x32, local copies, waits for them, and re-layouts: 6.04 us -> 9.41 us
  transfers between devices with their start and end apart: 7 -> 4, of which waited for: 6 -> 3; matrix products, arithmetic and copies ran while one was open for 3% -> 3% of each run, Pallas kernels for 5% -> 1%
where the time goes in v2:
time: 222 us; the launch traced here: 221 us
  blocking collectives  90 us (41%)
  waiting for transfers between devices  80.7 us (36%)
  starting transfers between devices  26.2 us (12%)
  local copies, waits for them, and re-layouts  11.2 us (5%)
  Pallas kernels  10.6 us (5%)
    all_to_all x1, blocking collectives, exchange(): return lax.all_to_all(pieces, axis, split_axis=0, concat_axis=0, tiled=True)  90 us
    all_to_all x4, waiting for transfers between devices, exchange(): return lax.all_to_all(pieces, axis, split_axis=0, concat_axis=0, tiled=True)  80.7 us
    all_to_all x4, starting transfers between devices, exchange(): return lax.all_to_all(pieces, axis, split_axis=0, concat_axis=0, tiled=True)  26.2 us
    unnamed x32, local copies, waits for them, and re-layouts  9.41 us
    pallas_call x1, Pallas kernels, per_device(): call(functools.partial(attend_cache, heads), shape((shards, HALF, 5 * LAN...  5.1 us
  transfers between devices with their start and end apart: 4, of which 3 were waited for; matrix products, arithmetic and copies ran while one was open for 3% of the time, Pallas kernels for 1%

profile of v2, /device:TPU:33, one launch (start us, length us, event | category | flops | bytes accessed | tf_op | source)
XLA Modules:
  0.0 221.3 jit_solution(14945039004997131162)
XLA Ops:
  0.6 0.0 copy-start
  0.6 0.8 copy-done
  1.5 0.0 copy-start.2
  1.5 0.8 copy-done.2
  2.2 0.0 copy-start.3
  2.2 0.8 copy-done.3
  3.0 0.0 copy-start.4
  3.0 0.8 copy-done.4
  3.7 0.0 copy-start.5
  3.8 0.8 copy-done.5
  4.5 0.0 copy-start.6
  4.5 0.8 copy-done.6
  5.3 0.7 copy-done.8
  5.9 0.3 projection_parts.1
  6.2 90.0 %all_to_all.25.part_ref = bf16[32,4,1152]{2,1,0:T(4,128)(2,1)S(1)} all-to-all(bf16[32,4,1152]{2,1,0:T(4,128)(2,1)S(1)} %projection_parts.1), channel_id=1, replica_groups=mesh['grp'=2,'kv'=32,'tp'=8] {'kv'}, dimensions={0} | all-to-all | bytes 589824 | tf_op jit(solution)/shard_map/all_to_all | solution.py:277
  96.3 0.9 finish_projections.1.mine_ref
  97.1 4.8 %all-to-all-start.1 = ((bf16[32,8,384]{2,1,0:T(8,128)(2,1)}), bf16[32,8,384]{2,1,0:T(8,128)(2,1)S(1)}, u32[]{:S(2)}, u32[]{:S(2)}) async-start(bf16[32,8,384]{2,1,0:T(8,128)(2,1)} %finish_projections.1.mine_ref), calls=%async_computation.1 | async-start | bytes 393216 | tf_op jit(solution)/shard_map/all_to_all | solution.py:277
  101.9 0.0 copy-done.13
  101.9 0.0 copy-start.9
  101.9 0.0 copy-start.10
  102.0 1.7 copy_bitcast_fusion
  103.7 31.8 %all-to-all-done.1.query_ref.fresh_ref = bf16[32,8,384]{2,1,0:T(8,128)(2,1)S(1)} async-done(((bf16[32,8,384]{2,1,0:T(8,128)(2,1)}), bf16[32,8,384]{2,1,0:T(8,128)(2,1)S(1)}, u32[]{:S(2)}, u32[]{:S(2)}) %all-to-all-start.1) | async-done | bytes 196640 | tf_op jit(solution)/shard_map/all_to_all | solution.py:277
  135.4 0.0 copy-done.9
  135.4 0.0 copy-done.10
  135.4 5.1 %attend_cache.1 = bf16[32,4,640]{2,1,0:T(4,128)(2,1)} custom-call(bf16[32,8,384]{2,1,0:T(8,128)(2,1)S(1)} %all-to-all-done.1.query_ref.fresh_ref, bf16[2,8,256,128]{3,2,1,0:T(8,128)(2,1)S(1)} %get-tuple-element.12.keys_ref, bf16[2,8,256,128]{3,2,1,0:T(8,128)(2,1)S(1)} %get-tuple-element.11.values_ref, s32[8]{0:T(128)S(1)} %copy-done.9, s32[8]{0:T(128)S(1)} %copy-done.10), custom_call_target="tpu_custom_call" | custom-call | flops 67108864 | bytes 65536 | tf_op jit(solution)/shard_map/attend_cache/pallas_call | solution.py:327
  140.6 5.3 %all-to-all-start.2 = ((bf16[32,4,640]{2,1,0:T(4,128)(2,1)}), bf16[32,4,640]{2,1,0:T(4,128)(2,1)S(1)}, u32[]{:S(2)}, u32[]{:S(2)}) async-start(bf16[32,4,640]{2,1,0:T(4,128)(2,1)} %attend_cache.1), calls=%async_computation.2 | async-start | bytes 327680 | tf_op jit(solution)/shard_map/all_to_all | solution.py:277
  145.9 0.1 compare_and_fusion
  146.0 0.1 broadcast_subtract_fusion
  146.1 0.0 copy-done.7
  146.1 1.3 attend_tree.1.tree_ref
  147.4 27.1 %all-to-all-done.2.part_ref = bf16[32,4,640]{2,1,0:T(4,128)(2,1)S(1)} async-done(((bf16[32,4,640]{2,1,0:T(4,128)(2,1)}), bf16[32,4,640]{2,1,0:T(4,128)(2,1)S(1)}, u32[]{:S(2)}, u32[]{:S(2)}) %all-to-all-start.2) | async-done | bytes 163872 | tf_op jit(solution)/shard_map/all_to_all | solution.py:277
  174.5 0.0 copy-done.11
  174.5 0.0 copy-done.12
  174.5 1.6 join_blocks.1
  176.2 7.2 %all-to-all-start.3 = ((bf16[32,8,128]{2,1,0:T(8,128)(2,1)}), bf16[32,8,128]{2,1,0:T(8,128)(2,1)S(1)}, u32[]{:S(2)}, u32[]{:S(2)}) async-start(bf16[32,8,128]{2,1,0:T(8,128)(2,1)} %join_blocks.1), calls=%async_computation.3 | async-start | bytes 131072 | tf_op jit(solution)/shard_map/all_to_all | solution.py:277
  183.4 0.0 copy-start.1
  183.4 0.0 copy-start.14
  183.4 0.8 fusion
  184.2 21.8 %all-to-all-done.3.head_out_ref = bf16[32,8,128]{2,1,0:T(8,128)(2,1)S(1)} async-done(((bf16[32,8,128]{2,1,0:T(8,128)(2,1)}), bf16[32,8,128]{2,1,0:T(8,128)(2,1)S(1)}, u32[]{:S(2)}, u32[]{:S(2)}) %all-to-all-start.3) | async-done | bytes 65568 | tf_op jit(solution)/shard_map/all_to_all | solution.py:277
  206.1 0.0 copy-done.1
  206.1 0.8 project_out.1
  206.8 8.9 %all-to-all-start.4 = ((bf16[8,16,128]{2,1,0:T(8,128)(2,1)}), bf16[8,16,128]{2,1,0:T(8,128)(2,1)S(1)}, u32[]{:S(2)}, u32[]{:S(2)}) async-start(bf16[8,16,128]{2,1,0:T(8,128)(2,1)} %bitcast.4), calls=%async_computation.4 | async-start | bytes 65536 | tf_op jit(solution)/shard_map/all_to_all | solution.py:277
  215.7 0.0 copy-done.14
  215.7 0.8 fusion.1
  216.6 2.0 copy.31
  218.6 2.0 copy.32
  220.7 0.0 all-to-all-done.4.part_ref
  220.7 0.6 add_groups.1
  (10 shorter events, 0.1 us)
Async XLA Ops:
  0.6 0.8 copy-start
  1.5 0.8 copy-start.2
  2.2 0.8 copy-start.3
  3.0 0.8 copy-start.4
  3.7 0.8 copy-start.5
  4.5 0.8 copy-start.6
  5.3 0.7 copy-start.8
  5.9 96.0 %copy-start.13 = (bf16[8,256,2,128]{3,2,1,0:T(2,128)(2,1)S(1)}, bf16[8,256,2,128]{3,2,1,0:T(2,128)(2,1)}, u32[]{:S(2)}) copy-start(bf16[8,256,2,128]{3,2,1,0:T(2,128)(2,1)} %param.25) | copy-start | bytes 3145732
  97.1 38.3 %all-to-all-start.1 = ((bf16[32,8,384]{2,1,0:T(8,128)(2,1)}), bf16[32,8,384]{2,1,0:T(8,128)(2,1)S(1)}, u32[]{:S(2)}, u32[]{:S(2)}) async-start(bf16[32,8,384]{2,1,0:T(8,128)(2,1)} %finish_projections.1.mine_ref), calls=%async_computation.1 | async-start | bytes 393216 | tf_op jit(solution)/shard_map/all_to_all | solution.py:277
  101.9 33.5 %copy-start.9 = (s32[8]{0:T(128)S(1)}, s32[8]{0:T(128)}, u32[]{:S(2)}) copy-start(s32[8]{0:T(128)} %lengths_ref.1) | copy-start | bytes 100
  101.9 33.5 %copy-start.10 = (s32[8]{0:T(128)S(1)}, s32[8]{0:T(128)}, u32[]{:S(2)}) copy-start(s32[8]{0:T(128)} %accepted_ref.1) | copy-start | bytes 100
  135.4 10.6 %copy-start.7 = (s32[8,16]{1,0:T(8,128)S(1)}, s32[8,16]{1,0:T(8,128)}, u32[]{:S(2)}) copy-start(s32[8,16]{1,0:T(8,128)} %parents_ref.1) | copy-start | bytes 1540
  140.5 34.0 %copy-start.11 = (f32[2]{0:T(128)S(1)}, f32[2]{0:T(128)}, u32[]{:S(2)}) copy-start(f32[2]{0:T(128)} %lambdas_ref.1) | copy-start | bytes 28
  140.6 34.0 %copy-start.12 = (bf16[128]{0:T(256)(128)(2,1)S(1)}, bf16[128]{0:T(256)(128)(2,1)}, u32[]{:S(2)}) copy-start(bf16[128]{0:T(256)(128)(2,1)} %param.22) | copy-start | bytes 772
  140.6 34.0 %all-to-all-start.2 = ((bf16[32,4,640]{2,1,0:T(4,128)(2,1)}), bf16[32,4,640]{2,1,0:T(4,128)(2,1)S(1)}, u32[]{:S(2)}, u32[]{:S(2)}) async-start(bf16[32,4,640]{2,1,0:T(4,128)(2,1)} %attend_cache.1), calls=%async_computation.2 | async-start | bytes 327680 | tf_op jit(solution)/shard_map/all_to_all | solution.py:277
  176.2 29.9 %all-to-all-start.3 = ((bf16[32,8,128]{2,1,0:T(8,128)(2,1)}), bf16[32,8,128]{2,1,0:T(8,128)(2,1)S(1)}, u32[]{:S(2)}, u32[]{:S(2)}) async-start(bf16[32,8,128]{2,1,0:T(8,128)(2,1)} %join_blocks.1), calls=%async_computation.3 | async-start | bytes 131072 | tf_op jit(solution)/shard_map/all_to_all | solution.py:277
  183.4 22.7 %copy-start.1 = (bf16[256,128]{1,0:T(8,128)(2,1)S(1)}, bf16[256,128]{1,0:T(8,128)(2,1)}, u32[]{:S(2)}) copy-start(bf16[256,128]{1,0:T(8,128)(2,1)} %weight_ref.1) | copy-start | bytes 196612
  183.4 32.4 %copy-start.14 = (bf16[8,256,2,128]{3,2,1,0:T(2,128)(2,1)S(1)}, bf16[8,256,2,128]{3,2,1,0:T(2,128)(2,1)}, u32[]{:S(2)}) copy-start(bf16[8,256,2,128]{3,2,1,0:T(2,128)(2,1)} %param.26) | copy-start | bytes 3145732
  206.8 13.8 %all-to-all-start.4 = ((bf16[8,16,128]{2,1,0:T(8,128)(2,1)}), bf16[8,16,128]{2,1,0:T(8,128)(2,1)S(1)}, u32[]{:S(2)}, u32[]{:S(2)}) async-start(bf16[8,16,128]{2,1,0:T(8,128)(2,1)} %bitcast.4), calls=%async_computation.4 | async-start | bytes 65536 | tf_op jit(solution)/shard_map/all_to_all | solution.py:277
